TPU v7x, 32 devices: a whole 2x2x4 slice. The times are simulated.
32 devices in a mesh: fs: 16 (over z, y, x), tp: 2 (over core).
Axes of the slice: x: 2, y: 2, z: 4, core: 2. Of those that a mesh axis runs over, the one named last changes fastest.
Arguments:
- block_input: bfloat16 [16384, 2048], P('fs'), may hold values from -6 to 6
- value_cotangent: bfloat16 [16384, 1024], P('fs', 'tp'), may hold values from -6 to 6
- mixed_output: bfloat16 [16384, 1024], P('fs', 'tp'), may hold values from -6 to 6
- output_cotangent: bfloat16 [16384, 2048], P('fs'), may hold values from -6 to 6
- value_weight: float32 [2048, 1024], P('fs', 'tp'), may hold values from -0.125 to 0.125
- output_weight: float32 [1024, 2048], P('tp', 'fs'), may hold values from -0.1875 to 0.1875
- value_basis: bfloat16 [2048, 384], P('fs'), may hold values from -0.125 to 0.125
- output_basis: bfloat16 [2048, 384], P('fs'), may hold values from -0.125 to 0.125
- value_mean: float32 [384, 1024], P(None, 'tp'), may hold values from -4 to 4
- value_square: float32 [384, 1024], P(None, 'tp'), may hold values from 0.3 to 2
- output_mean: float32 [1024, 384], P('tp'), may hold values from -4 to 4
- output_square: float32 [1024, 384], P('tp'), may hold values from 0.3 to 2
Outputs:
- value_next: float32 [2048, 1024], P('fs', 'tp')
- value_copy: bfloat16 [2048, 1024], P(None, 'tp')
- value_step: float32 [2048, 1024], P('fs', 'tp')
- value_mean_next: float32 [384, 1024], P(None, 'tp')
- value_square_next: float32 [384, 1024], P(None, 'tp')
- output_next: float32 [1024, 2048], P('tp', 'fs')
- output_copy: bfloat16 [1024, 2048], P('tp')
- output_step: float32 [1024, 2048], P('tp', 'fs')
- output_mean_next: float32 [1024, 384], P('tp')
- output_square_next: float32 [1024, 384], P('tp')
All inputs are finite; a program needn't handle non-finite values.
Results may differ from a plain program's by a relative error of at most 0.002.
Values may be sent and summed in bfloat16 or wider, within the bound.
A program may use at most 64 MiB of HBM per device.

v0:
```python
import functools
import math

import jax
import jax.numpy as jnp
from jax import lax
from jax.experimental import pallas as pl
from jax.experimental.pallas import tpu as pltpu
from jax.sharding import PartitionSpec as P

MESH = pl.DeviceIdType.MESH
VALUE_RATE = 125.0 / 0.125
OUTPUT_RATE = 125.0 / 0.1875
LOW_RATE = 124.0
BLOCK_LANES = 256
TOKEN_TILE = 256


def split_fs(n):
    inner = 2 if n % 2 == 0 else 1
    middle = 2 if n % (2 * inner) == 0 else 1
    return n // (inner * middle), middle, inner


class Place:
    def __init__(self, n):
        self.sizes = split_fs(n)
        self.me = lax.axis_index("fs")
        self.core = lax.axis_index("tp")
        self.par = lax.rem(self.core, 2)
        _, b, c = self.sizes
        self.z = self.me // (b * c)
        self.y = lax.rem(self.me // c, b)
        self.x = lax.rem(self.me, c)

    def at(self, dz, ds, dt, par=None):
        a, b, c = self.sizes
        par = self.par if par is None else par
        dy = ds * (1 - par) + dt * par
        dx = ds * par + dt * (1 - par)
        z = lax.rem(self.z + dz + a, a)
        y = lax.rem(self.y + dy, b)
        x = lax.rem(self.x + dx, c)
        return (z * b + y) * c + x


class Gather:
    def __init__(self, place, slots, send, recv):
        self.p, self.slots, self.send, self.recv = place, slots, send, recv
        self.a = place.sizes[0]
        self.started = []

    def copy(self, j, src, to, sid, rid):
        ref = self.slots[j](src)
        return pltpu.make_async_remote_copy(
            src_ref=ref, dst_ref=ref, send_sem=self.send.at[j, sid], recv_sem=self.recv.at[j, rid],
            device_id={"fs": to}, device_id_type=MESH)

    def rel(self, dz, ds, dt):
        return (dz * 2 + ds) * 2 + dt

    def go(self, j, src, to, sid, rid):
        c = self.copy(j, src, to, sid, rid)
        c.start()
        self.started.append(c)

    def arrive(self, dz, ds, dt):
        for j in range(len(self.slots)):
            src = self.p.at(-dz, ds, dt)
            self.copy(j, src, self.p.me, 0, self.rel(dz, ds, dt)).wait_recv()

    def to_s(self, dz):
        for j in range(len(self.slots)):
            self.go(j, self.p.at(-dz, 0, 0), self.p.at(0, 1, 0), self.a + dz, self.rel(dz, 1, 0))

    def to_t(self, dz, ds):
        for j in range(len(self.slots)):
            self.go(j, self.p.at(-dz, ds, 0), self.p.at(0, 0, 1), 2 * self.a + dz * 2 + ds, self.rel(dz, ds, 1))

    def begin(self):
        self.begin_z()
        self.begin_st()

    def begin_z(self):
        for dz in range(1, self.a):
            for j in range(len(self.slots)):
                self.go(j, self.p.me, self.p.at(dz, 0, 0), dz, self.rel(dz, 0, 0))

    def begin_st(self):
        self.to_s(0)
        self.to_t(0, 0)

    def stage_z(self, seen=lambda *k: None):
        for dz in range(1, self.a):
            self.arrive(dz, 0, 0)
            self.to_s(dz)
            self.to_t(dz, 0)
            seen(dz, 0, 0)

    def stage_s(self, seen=lambda *k: None):
        for dz in range(self.a):
            self.arrive(dz, 1, 0)
            self.to_t(dz, 1)
            seen(dz, 1, 0)

    def stage_t(self, seen=lambda *k: None):
        for dz in range(self.a):
            for ds in range(2):
                self.arrive(dz, ds, 1)
                seen(dz, ds, 1)

    def finish(self):
        for c in self.started:
            c.wait_send()


def exchange(n, scaling, x_hbm, v_hbm, m_hbm, o_hbm, vb_ref, ob_ref, vw_ref, ow_ref,
             bases, wv, wo, low_v, low_o, sums,
             vw32, ow32, x_ref, v_ref, m_ref, o_ref, acc_v, acc_o, part_v, part_o, got_v, got_o,
             load_sem, own_sem, b_send, b_recv, c_send, c_recv, w_send, w_recv, l_send, l_recv, r_send, r_recv, q_send, q_recv):
    p = Place(n)
    a = p.sizes[0]
    par, me = p.par, p.me
    loads = [pltpu.make_async_copy(s, d, load_sem.at[i]) for i, (s, d) in enumerate(
        ((vw_ref, vw32), (ow_ref, ow32), (x_hbm, x_ref), (v_hbm, v_ref), (o_hbm, o_ref), (m_hbm, m_ref)))]
    own = [pltpu.make_async_copy(s, d, own_sem.at[i]) for i, (s, d) in enumerate(
        ((vb_ref, bases.at[0, me]), (ob_ref, bases.at[1, me])))]
    for c in own + loads:
        c.start()
    partner = p.core + 1 - 2 * par
    barrier = pltpu.get_barrier_semaphore()
    peers = [p.at(dz, 0, 0) for dz in range(1, a)] + [p.at(0, 1, 0), p.at(0, 0, 1)]
    for to in peers:
        pl.semaphore_signal(barrier, inc=1, device_id={"fs": to}, device_id_type=MESH)
    cores = lax.axis_size("tp")
    siblings = [lax.rem(p.core + d, cores) for d in range(1, cores)]
    for to in siblings:
        pl.semaphore_signal(barrier, inc=1, device_id={"tp": to}, device_id_type=MESH)
    pl.semaphore_wait(barrier, len(peers) + len(siblings))
    for c in own:
        c.wait()

    crossed = []

    def cross(dz, ds, dt):
        k = (dz * 2 + ds) * 2 + dt
        ref = bases.at[par, p.at(-dz, ds, dt)]
        c = pltpu.make_async_remote_copy(
            src_ref=ref, dst_ref=ref, send_sem=c_send.at[k], recv_sem=c_recv.at[k],
            device_id={"tp": partner}, device_id_type=MESH)
        c.start()
        crossed.append(c)

    gb = Gather(p, [lambda i: bases.at[par, i]], b_send, b_recv)
    gb.begin()
    for c in loads[:2]:
        c.wait()
    wv[me] = jnp.exp2(VALUE_RATE * vw32[...]).astype(wv.dtype)
    wo[me] = jnp.exp2(OUTPUT_RATE * ow32[...]).astype(wo.dtype)
    gb.stage_z(cross)
    gw = Gather(p, [lambda i: wv.at[i], lambda i: wo.at[i]], w_send, w_recv)
    gw.begin_z()
    gb.stage_s(cross)
    gb.stage_t(cross)
    gw.begin_st()
    for dz in range(a):
        for ds in range(2):
            for dt in range(2):
                k = (dz * 2 + ds) * 2 + dt
                if k:
                    ref = bases.at[1 - par, p.at(-dz, ds, dt, 1 - par)]
                    pltpu.make_async_remote_copy(
                        src_ref=ref, dst_ref=ref, send_sem=c_send.at[k], recv_sem=c_recv.at[k],
                        device_id={"tp": partner}, device_id_type=MESH).wait_recv()
    for c in loads[2:]:
        c.wait()

    depth, rank = bases.shape[2], bases.shape[3]
    tokens = x_ref.shape[0]
    tile = math.gcd(tokens, TOKEN_TILE)
    acc_v[...] = jnp.zeros_like(acc_v)
    acc_o[...] = jnp.zeros_like(acc_o)
    whole_v = bases[0].reshape(n * depth, rank)
    whole_o = bases[1].reshape(n * depth, rank)
    first = (((0,), (0,)), ((), ()))

    def halves(value):
        high = value.astype(jnp.bfloat16)
        return high, (value - high.astype(jnp.float32)).astype(jnp.bfloat16)

    @pl.loop(0, tokens // tile)
    def _(step):
        rows = pl.ds(pl.multiple_of(step * tile, tile), tile)
        cot = v_ref[rows, :]
        for half in halves(jnp.dot(x_ref[rows, :], whole_v, preferred_element_type=jnp.float32)):
            acc_v[...] += lax.dot_general(half, cot, first, preferred_element_type=jnp.float32)
        mixed = m_ref[rows, :]
        for half in halves(jnp.dot(o_ref[rows, :], whole_o, preferred_element_type=jnp.float32)):
            acc_o[...] += lax.dot_general(mixed, half, first, preferred_element_type=jnp.float32)

    parts, gots = (part_v, part_o), (got_v, got_o)
    for part, acc in ((part_v, acc_v), (part_o, acc_o)):
        high = part.shape[1]
        for i in range(n):
            part[i] = acc[i * high:(i + 1) * high, :] * scaling

    sent = []

    def hand(block, to, slot):
        for j in range(2):
            c = pltpu.make_async_remote_copy(
                src_ref=parts[j].at[block], dst_ref=gots[j].at[slot],
                send_sem=r_send.at[j, slot], recv_sem=r_recv.at[j, slot],
                device_id={"fs": to}, device_id_type=MESH)
            c.start()
            sent.append(c)

    def take(block, slot):
        for j in range(2):
            pltpu.make_async_remote_copy(
                src_ref=parts[j].at[block], dst_ref=gots[j].at[slot],
                send_sem=r_send.at[j, slot], recv_sem=r_recv.at[j, slot],
                device_id={"fs": me}, device_id_type=MESH).wait_recv()
            parts[j][block] += gots[j][slot]

    order = list(range(1, a)) + [0]
    for dz in order:
        for ds in (1, 0):
            hand(p.at(dz, ds, 1), p.at(0, 0, 1), dz * 2 + ds)
    gw.stage_z()
    for dz in order:
        take(p.at(dz, 1, 0), dz * 2 + 1)
        hand(p.at(dz, 1, 0), p.at(0, 1, 0), 2 * a + dz)
        take(p.at(dz, 0, 0), dz * 2)
    for dz in order:
        take(p.at(dz, 0, 0), 2 * a + dz)
        if dz:
            hand(p.at(dz, 0, 0), p.at(dz, 0, 0), 3 * a + dz)
    for dz in range(1, a):
        take(me, 3 * a + dz)
    mine_v, mine_o = part_v[me], part_o[me]

    def one(reduce, value):
        return reduce(reduce(value, axis=1, keepdims=True), axis=0, keepdims=True)

    top = jnp.maximum(one(jnp.max, jnp.abs(mine_v)), one(jnp.max, jnp.abs(mine_o)))
    top = jnp.maximum(top * 1.01, 1e-30).astype(low_v.dtype)
    square = one(jnp.sum, mine_v * mine_v) + one(jnp.sum, mine_o * mine_o)
    rate = LOW_RATE / top.astype(jnp.float32)
    high = mine_v.shape[0]
    pad = low_v.shape[1] - high
    square_high, square_low = halves(square)
    row = lax.broadcasted_iota(jnp.int32, (pad, mine_v.shape[1]), 0)
    extra = jnp.where(row == 0, top.astype(jnp.float32), jnp.where(
        row == 1, square_high.astype(jnp.float32), square_low.astype(jnp.float32)))
    low_v[me] = jnp.concatenate([jnp.exp2(rate * mine_v), extra], axis=0).astype(low_v.dtype)
    low_o[me] = jnp.exp2(rate * mine_o).astype(low_o.dtype)
    gl = Gather(p, [lambda i: low_v.at[i], lambda i: low_o.at[i]], l_send, l_recv)
    gl.begin()
    gw.stage_s()
    gl.stage_z()
    gl.stage_s()
    gl.stage_t()
    total = jnp.zeros((1, 128), jnp.float32)
    for i in range(n):
        tail = low_v[i].astype(jnp.float32)
        total += tail[high + 1:high + 2, :128] + tail[high + 2:high + 3, :128]
    sums[p.core] = jnp.broadcast_to(total, sums.shape[1:])
    for d, to in enumerate(siblings):
        c = pltpu.make_async_remote_copy(
            src_ref=sums.at[p.core], dst_ref=sums.at[p.core], send_sem=q_send.at[d], recv_sem=q_recv.at[d],
            device_id={"tp": to}, device_id_type=MESH)
        c.start()
        sent.append(c)
    gw.stage_t()
    for d in range(cores - 1):
        ref = sums.at[lax.rem(p.core - d - 1 + cores, cores)]
        pltpu.make_async_remote_copy(
            src_ref=ref, dst_ref=ref, send_sem=q_send.at[d], recv_sem=q_recv.at[d],
            device_id={"tp": partner}, device_id_type=MESH).wait_recv()
    for c in crossed + sent:
        c.wait_send()
    gb.finish()
    gw.finish()
    gl.finish()


def low_and_weights(block_input, value_cotangent, mixed_output, output_cotangent, value_basis, output_basis, value_weight, output_weight):
    n = lax.axis_size("fs")
    depth, rank = value_basis.shape
    tokens, width = value_cotangent.shape
    wide = block_input.shape[1]
    a = split_fs(n)[0]
    cores = lax.axis_size("tp")
    scaling = 1.0 / math.sqrt(tokens * n)
    f32, b16 = jnp.float32, jnp.bfloat16
    rv, ro = rank // n, width // n
    vmem = pl.BlockSpec(memory_space=pltpu.VMEM)
    hbm = pl.BlockSpec(memory_space=pl.ANY)
    dma = pltpu.SemaphoreType.DMA
    return pl.pallas_call(
        functools.partial(exchange, n, scaling),
        out_shape=(
            jax.ShapeDtypeStruct((2, n, depth, rank), b16),
            jax.ShapeDtypeStruct((n,) + value_weight.shape, b16),
            jax.ShapeDtypeStruct((n,) + output_weight.shape, b16),
            jax.ShapeDtypeStruct((n, (rv + 18) // 16 * 16, width), b16),
            jax.ShapeDtypeStruct((n, ro, rank), b16),
            jax.ShapeDtypeStruct((cores, 8, 128), f32),
        ),
        in_specs=[hbm] * 4 + [hbm] * 4,
        out_specs=[vmem] * 6,
        scratch_shapes=[
            pltpu.VMEM(value_weight.shape, f32), pltpu.VMEM(output_weight.shape, f32),
            pltpu.VMEM((tokens, wide), b16), pltpu.VMEM((tokens, width), b16),
            pltpu.VMEM((tokens, width), b16), pltpu.VMEM((tokens, wide), b16),
            pltpu.VMEM((rank, width), f32), pltpu.VMEM((width, rank), f32),
            pltpu.VMEM((n, rv, width), f32), pltpu.VMEM((n, ro, rank), f32),
            pltpu.VMEM((4 * a, rv, width), f32), pltpu.VMEM((4 * a, ro, rank), f32),
            dma((6,)), dma((2,)),
            dma((1, 4 * a)), dma((1, 4 * a)), dma((4 * a,)), dma((4 * a,)),
            dma((2, 4 * a)), dma((2, 4 * a)), dma((2, 4 * a)), dma((2, 4 * a)), dma((2, 4 * a)), dma((2, 4 * a)),
            dma((cores,)), dma((cores,)),
        ],
        compiler_params=pltpu.CompilerParams(
            collective_id=0, has_side_effects=True, vmem_limit_bytes=60 * 1024 * 1024),
    )(block_input, value_cotangent, mixed_output, output_cotangent, value_basis, output_basis, value_weight, output_weight)


def split_norm(norm, norms):
    norms[0] = norm.astype(jnp.bfloat16)
    norms[1] = (norm - norms[0].astype(jnp.float32)).astype(jnp.bfloat16)


def value_steps(basis, norms):
    return (jnp.dot(basis, norms[0], preferred_element_type=jnp.float32)
            + jnp.dot(basis, norms[1], preferred_element_type=jnp.float32))


def output_steps(basis, norms):
    last = (((1,), (1,)), ((), ()))
    return (lax.dot_general(norms[0], basis, last, preferred_element_type=jnp.float32)
            + lax.dot_general(norms[1], basis, last, preferred_element_type=jnp.float32))


def epilogue(entries, low_v, low_o, sums, vm, vs, om, os, vw, ow, vb, ob, bases, wv, wo,
             v_next, v_copy, v_step, vm_next, vs_next, o_next, o_copy, o_step, om_next, os_next,
             norms_v, norms_o):
    @pl.when(pl.program_id(0) == 0)
    def _():
        n, high, high_o = low_v.shape[0], vm.shape[0] // low_v.shape[0], low_o.shape[1]
        total = sums[0, :1, :1]
        for i in range(1, sums.shape[0]):
            total += sums[i, :1, :1]
        clip = 1.0 / jnp.sqrt(1.0 + total / entries)
        for i in range(n):
            code = low_v[i].astype(jnp.float32)
            rate = clip * code[high:high + 1, :1] * (1.0 / LOW_RATE)
            for part, at, mean, square, mean_next, square_next in (
                (code[:high], slice(i * high, (i + 1) * high), vm, vs, vm_next, vs_next),
                (low_o[i].astype(jnp.float32), slice(i * high_o, (i + 1) * high_o), om, os, om_next, os_next),
            ):
                scaled = rate * jnp.log2(part)
                mean_next[at] = 0.8 * mean[at] + 0.2 * scaled
                square_next[at] = 0.9 * square[at] + 0.1 * scaled * scaled
        split_norm(vm_next[...] / jnp.sqrt(vs_next[...] + 0.1), norms_v)
        split_norm(om_next[...] / jnp.sqrt(os_next[...] + 0.1), norms_o)
        v_step[...] = value_steps(vb[...], norms_v)
        v_next[...] = vw[...] - 0.02 * v_step[...]
        o_step[...] = output_steps(ob[...], norms_o)
        o_next[...] = ow[...] - 0.02 * o_step[...]

    count, rows, cols = wv.shape[0], wv.shape[1], wo.shape[2]
    for k in range(count):
        old = jnp.log2(wv[k].astype(jnp.float32)) * (1.0 / VALUE_RATE)
        v_copy[k * rows:(k + 1) * rows, :] = (old - 0.02 * value_steps(bases[0, k], norms_v)).astype(v_copy.dtype)
        old = jnp.log2(wo[k].astype(jnp.float32)) * (1.0 / OUTPUT_RATE)
        o_copy[:, k * cols:(k + 1) * cols] = (old - 0.02 * output_steps(bases[1, k], norms_o)).astype(o_copy.dtype)


def on_device(
    block_input,
    value_cotangent,
    mixed_output,
    output_cotangent,
    value_weight,
    output_weight,
    value_basis,
    output_basis,
    value_mean,
    value_square,
    output_mean,
    output_square,
):
    n = lax.axis_size("fs")
    depth, rank = value_basis.shape
    width = value_cotangent.shape[1]
    bases, wv, wo, low_v, low_o, sums = low_and_weights(
        block_input, value_cotangent, mixed_output, output_cotangent, value_basis, output_basis,
        value_weight, output_weight)
    entries = 2.0 * rank * width * lax.axis_size("tp")
    count = math.gcd(n, max(1, BLOCK_LANES // depth))

    def full(array):
        return pl.BlockSpec(array.shape, lambda i: (0,) * array.ndim)

    f32, b16 = jnp.float32, jnp.bfloat16
    small = [low_v, low_o, sums, value_mean, value_square, output_mean, output_square,
             value_weight, output_weight, value_basis, output_basis]
    v_row, v_small = jax.ShapeDtypeStruct((depth, width), f32), jax.ShapeDtypeStruct((rank, width), f32)
    o_row, o_small = jax.ShapeDtypeStruct((width, depth), f32), jax.ShapeDtypeStruct((width, rank), f32)
    v_all, o_all = jax.ShapeDtypeStruct((n * depth, width), b16), jax.ShapeDtypeStruct((width, n * depth), b16)
    return pl.pallas_call(
        functools.partial(epilogue, entries),
        grid=(n // count,),
        out_shape=(v_row, v_all, v_row, v_small, v_small, o_row, o_all, o_row, o_small, o_small),
        in_specs=[full(array) for array in small] + [
            pl.BlockSpec((2, count, depth, rank), lambda i: (0, i, 0, 0)),
            pl.BlockSpec((count, depth, width), lambda i: (i, 0, 0)),
            pl.BlockSpec((count, width, depth), lambda i: (i, 0, 0)),
        ],
        out_specs=[
            full(v_row), pl.BlockSpec((count * depth, width), lambda i: (i, 0)), full(v_row), full(v_small), full(v_small),
            full(o_row), pl.BlockSpec((width, count * depth), lambda i: (0, i)), full(o_row), full(o_small), full(o_small),
        ],
        scratch_shapes=[pltpu.VMEM((2, rank, width), b16), pltpu.VMEM((2, width, rank), b16)],
        compiler_params=pltpu.CompilerParams(
            dimension_semantics=("arbitrary",), vmem_limit_bytes=60 * 1024 * 1024),
    )(*small, bases, wv, wo)


def solution(mesh):
    placed = (
        P("fs", None),
        P("fs", "tp"),
        P("fs", "tp"),
        P("fs", None),
        P("fs", "tp"),
        P("tp", "fs"),
        P("fs", None),
        P("fs", None),
        P(None, "tp"),
        P(None, "tp"),
        P("tp", None),
        P("tp", None),
    )
    return jax.shard_map(
        on_device,
        mesh=mesh,
        in_specs=placed,
        out_specs=(
            P("fs", "tp"),
            P(None, "tp"),
            P("fs", "tp"),
            P(None, "tp"),
            P(None, "tp"),
            P("tp", "fs"),
            P("tp", None),
            P("tp", "fs"),
            P("tp", None),
            P("tp", None),
        ),
        check_vma=False,
    )
```

profile of v0, /device:TPU:9, one launch (start us, length us, event | category | flops | bytes accessed | tf_op | source)
XLA Modules:
  0.0 112.6 jit_solution(11443222307394364838)
XLA Ops:
  0.6 97.6 %shard_map.195 = (bf16[2,16,128,384]{3,2,1,0:T(8,128)(2,1)}, bf16[16,128,512]{2,1,0:T(8,128)(2,1)}, bf16[16,512,128]{2,1,0:T(8,128)(2,1)}, bf16[16,32,512]{2,1,0...) custom-call(bf16[1024,2048]{1,0:T(8,128)(2,1)} %x_hbm.1, bf16[1024,512]{1,0:T(8,128)(2,1)} %v_hbm.1, ...), custom_call_target="tpu_custom_call" | custom-call | tf_op jit(solution)/shard_map/pallas_call | solution.py:301
  98.3 14.3 %shard_map.196 = (f32[128,512]{1,0:T(8,128)}, bf16[2048,512]{1,0:T(8,128)(2,1)}, f32[128,512]{1,0:T(8,128)}, f32[384,512]{1,0:T(8,128)}, f32[384,512]{1,0:T(8,12...) custom-call(bf16[16,32,512]{2,1,0:T(8,128)(2,1)} %get-tuple-element., ...), custom_call_target="tpu_custom_call" | custom-call | tf_op jit(solution)/shard_map/pallas_call | solution.py:413
where the time goes:
time: 113 us
  Pallas kernels  112 us (99%)
    pallas_call x1, Pallas kernels, low_and_weights(): pl.pallas_call(functools.partial(exchange, n, scaling), out_shape=(jax.Sh...  97.6 us
    pallas_call x1, Pallas kernels, on_device(): pl.pallas_call(functools.partial(epilogue, entries), grid=(n // count,),...  14.3 us

commit v1 on v0

v1 whole, which is shorter than its diff:
```python
import functools
import math

import jax
import jax.numpy as jnp
from jax import lax
from jax.experimental import pallas as pl
from jax.experimental.pallas import tpu as pltpu
from jax.sharding import PartitionSpec as P

MESH = pl.DeviceIdType.MESH
VALUE_RATE = 125.0 / 0.125
OUTPUT_RATE = 125.0 / 0.1875
LOW_RATE = 124.0
BLOCK_LANES = 256
TOKEN_TILE = 256
FIRST = (((0,), (0,)), ((), ()))
LAST = (((1,), (1,)), ((), ()))


def split_fs(n):
    inner = 2 if n % 2 == 0 else 1
    middle = 2 if n % (2 * inner) == 0 else 1
    return n // (inner * middle), middle, inner


class Place:
    def __init__(self, n):
        self.sizes = split_fs(n)
        self.me = lax.axis_index("fs")
        self.core = lax.axis_index("tp")
        self.par = lax.rem(self.core, 2)
        self.partner = self.core + 1 - 2 * self.par
        a, b, c = self.sizes
        self.z = self.me // (b * c)
        self.y = lax.rem(self.me // c, b)
        self.x = lax.rem(self.me, c)
        self.planes = [self.near(i) for i in range(a)]

    def near(self, i):
        a = self.sizes[0]
        low = jnp.minimum(self.z, a - 1 - self.z)
        side = self.z - (i + 1) // 2 if i % 2 else self.z + i // 2
        return jnp.where(2 * low >= i, side, jnp.where(self.z <= a - 1 - self.z, i, a - 1 - i))

    def on(self, z, ds, dt, par=None):
        a, b, c = self.sizes
        par = self.par if par is None else par
        y = lax.rem(self.y + ds * (1 - par) + dt * par, b)
        x = lax.rem(self.x + ds * par + dt * (1 - par), c)
        return (z * b + y) * c + x

    def at(self, dz, ds, dt):
        return self.on(lax.rem(self.z + dz, self.sizes[0]), ds, dt)


class Gather:
    def __init__(self, place, slot, send, recv, line=False, plane_first=False, seen=None):
        self.p, self.slot, self.send, self.recv = place, slot, send, recv
        self.line, self.plane_first, self.seen = line, plane_first, seen or (lambda *k: None)
        self.a = place.sizes[0]
        self.started = []

    def copy(self, src, ds, to, kind, sid, rid):
        ref = self.slot(self.p.on(src, ds, 0))
        return pltpu.make_async_remote_copy(
            src_ref=ref, dst_ref=ref, send_sem=self.send.at[kind, sid], recv_sem=self.recv.at[rid],
            device_id={"fs": to}, device_id_type=MESH)

    def go(self, src, ds, to, kind, sid, rid, when=None):
        def make():
            return self.copy(src, ds, to, kind, sid, rid)

        self.started.append((make, when))
        if when is None:
            make().start()
        else:
            @pl.when(when)
            def _():
                make().start()

    def came(self, src, ds, dt):
        ref = self.slot(self.p.on(src, ds, dt))
        pltpu.make_async_remote_copy(
            src_ref=ref, dst_ref=ref, send_sem=self.send.at[0, 0], recv_sem=self.recv.at[(src * 2 + ds) * 2 + dt],
            device_id={"fs": self.p.me}, device_id_type=MESH).wait_recv()

    def to_s(self, src):
        self.go(src, 0, self.p.on(self.p.z, 1, 0), 2, src * 2, (src * 2 + 1) * 2)

    def to_t(self, src, ds):
        self.go(src, ds, self.p.on(self.p.z, 0, 1), 3, src * 2 + ds, (src * 2 + ds) * 2 + 1)

    def begin_z(self, ds=0):
        z, rid = self.p.z, (self.p.z * 2 + ds) * 2
        if self.line:
            self.go(z, ds, self.p.on(z + 1, 0, 0), 0, z * 2 + ds, rid, z < self.a - 1)
            self.go(z, ds, self.p.on(z - 1, 0, 0), 1, z * 2 + ds, rid, z > 0)
        else:
            for dz in range(1, self.a):
                self.go(z, ds, self.p.at(dz, 0, 0), 0, dz * 2 + ds, rid)

    def begin_st(self):
        self.to_s(self.p.z)
        self.to_t(self.p.z, 0)
        self.seen(self.p.z, 0, 0)

    def begin(self):
        self.begin_z()
        self.begin_st()

    def near_s(self):
        self.came(self.p.z, 1, 0)
        self.begin_z(1)
        self.to_t(self.p.z, 1)
        self.seen(self.p.z, 1, 0)

    def z(self, k, ds=0):
        if k >= self.a:
            return
        src, z = self.p.planes[k], self.p.z
        self.came(src, ds, 0)
        if self.line:
            up = src < z
            to = jnp.clip(jnp.where(up, z + 1, z - 1), 0, self.a - 1)
            inside = jnp.where(up, z + 1, self.a - z) < self.a
            self.go(src, ds, self.p.on(to, 0, 0), 0, src * 2 + ds, (src * 2 + ds) * 2, inside)
        if not self.plane_first:
            self.to_s(src)
        self.to_t(src, ds)
        self.seen(src, ds, 0)

    def s(self, k):
        if k < self.a:
            src = self.p.planes[k]
            self.came(src, 1, 0)
            self.to_t(src, 1)
            self.seen(src, 1, 0)

    def t(self, k):
        if k < self.a:
            for ds in range(2):
                self.came(self.p.planes[k], ds, 1)
                self.seen(self.p.planes[k], ds, 1)

    def last(self):
        for k in range(self.a):
            self.t(k)

    def finish(self):
        for make, when in self.started:
            if when is None:
                make().wait_send()
            else:
                @pl.when(when)
                def _():
                    make().wait_send()


class Bases(Gather):
    def __init__(self, place, ref, send, recv, c_send, c_recv):
        half = ref.shape[1] // 2
        rows = [pl.ds(pl.multiple_of(side * half, half), half) for side in (place.par, 1 - place.par)]
        super().__init__(place, lambda i: ref.at[i, rows[0]], send, recv, line=False, seen=self.cross)
        self.other = lambda i: ref.at[i, rows[1]]
        self.c_send, self.c_recv = c_send, c_recv
        self.crossed = []

    def over(self, ref, k):
        return pltpu.make_async_remote_copy(
            src_ref=ref, dst_ref=ref, send_sem=self.c_send.at[k], recv_sem=self.c_recv.at[k],
            device_id={"tp": self.p.partner}, device_id_type=MESH)

    def cross(self, src, ds, dt):
        c = self.over(self.slot(self.p.on(src, ds, dt)), (src * 2 + ds) * 2 + dt)
        c.start()
        self.crossed.append(c)

    def whole(self):
        for src in range(self.a):
            for ds in range(2):
                for dt in range(2):
                    self.over(self.other(self.p.on(src, ds, dt, 1 - self.p.par)), (src * 2 + ds) * 2 + dt).wait_recv()

    def finish(self):
        super().finish()
        for c in self.crossed:
            c.wait_send()


def halves(value):
    high = value.astype(jnp.bfloat16)
    return high, (value - high.astype(jnp.float32)).astype(jnp.bfloat16)


def one(reduce, value):
    return reduce(reduce(value, axis=1, keepdims=True), axis=0, keepdims=True)


def bound(values):
    top = jnp.maximum(one(jnp.max, jnp.abs(values)) * 1.01, 1e-30)
    return top.astype(jnp.bfloat16).astype(jnp.float32)


def encode(values, entries, rows):
    row = lax.broadcasted_iota(jnp.int32, (rows - values.shape[0], values.shape[1]), 0)
    extra = jnp.zeros(row.shape, jnp.float32)
    for k, entry in enumerate(entries):
        extra = jnp.where(row == k, entry.astype(jnp.float32), extra)
    return jnp.concatenate([jnp.exp2((LOW_RATE / entries[0]) * values), extra], axis=0).astype(jnp.bfloat16)


def decode(code, high):
    top = code[high:high + 1].astype(jnp.float32)
    return top * (1.0 / LOW_RATE) * jnp.log2(code[:high].astype(jnp.float32)), top


class Scatter:
    def __init__(self, place, part, code, got, send, recv):
        self.p, self.part, self.code, self.got, self.send, self.recv = place, part, code, got, send, recv
        self.a = place.sizes[0]
        self.order = list(range(1, self.a)) + [0]
        self.started = []

    def copy(self, block, to, slot):
        return pltpu.make_async_remote_copy(
            src_ref=self.code.at[block], dst_ref=self.got.at[slot],
            send_sem=self.send.at[slot], recv_sem=self.recv.at[slot],
            device_id={"fs": to}, device_id_type=MESH)

    def hand(self, block, to, slot, top):
        self.code[block] = encode(self.part[block], (top,), self.code.shape[1])
        c = self.copy(block, to, slot)
        c.start()
        self.started.append(c)

    def take(self, block, slot):
        self.copy(block, self.p.me, slot).wait_recv()
        value, top = decode(self.got[slot], self.part.shape[1])
        self.part[block] += value
        return top.astype(jnp.bfloat16).astype(jnp.float32)

    def grown(self, top):
        return top.astype(jnp.bfloat16).astype(jnp.float32)

    def give_t(self):
        n, high, width = self.part.shape
        self.top = jnp.broadcast_to(bound(self.part[...].reshape(n * high, width)), (1, width))
        for dz in self.order:
            for ds in (1, 0):
                self.hand(self.p.at(dz, ds, 1), self.p.on(self.p.z, 0, 1), dz * 2 + ds, self.top)

    def turn_s(self, i):
        if i < self.a:
            dz = self.order[i]
            top = self.take(self.p.at(dz, 1, 0), dz * 2 + 1)
            if i == 0:
                self.top = self.grown(self.top + top)
            self.hand(self.p.at(dz, 1, 0), self.p.on(self.p.z, 1, 0), 2 * self.a + dz, self.top)
            self.take(self.p.at(dz, 0, 0), dz * 2)

    def turn_z(self, i):
        if i < self.a:
            dz = self.order[i]
            top = self.take(self.p.at(dz, 0, 0), 2 * self.a + dz)
            if i == 0:
                self.top = self.grown(self.top + top)
            if dz:
                self.hand(self.p.at(dz, 0, 0), self.p.at(dz, 0, 0), 3 * self.a + dz, self.top)

    def end(self):
        for dz in range(1, self.a):
            self.take(self.p.me, 3 * self.a + dz)

    def finish(self):
        for c in self.started:
            c.wait_send()


def twice(basis):
    return jnp.concatenate([basis, basis], axis=1)


def exchange(n, scaling, entries, x_hbm, v_hbm, m_hbm, o_hbm, vb_hbm, ob_hbm, vw_hbm, ow_hbm, vm_hbm, vs_hbm, om_hbm, os_hbm,
             v_next, v_copy, v_step, vm_next, vs_next, o_next, o_copy, o_step, om_next, os_next,
             bases, wv, wo, low, sums, vw, ow, x_ref, v_ref, m_ref, o_ref, vm, vs, om, os, part, code, got, small, norms_v, norms_o,
             load_sem, own_sem, b_send, b_recv, c_send, c_recv, w_send, w_recv, l_send, l_recv, r_send, r_recv, q_send, q_recv):
    p = Place(n)
    a, b, c = p.sizes
    par, me = p.par, p.me
    half = bases.shape[2] // 2
    mine = pl.ds(pl.multiple_of(par * half, half), half)
    own = [pltpu.make_async_copy(s.at[mine], bases.at[i, me, mine], own_sem.at[i]) for i, s in enumerate((vb_hbm, ob_hbm))]
    loads = [pltpu.make_async_copy(s, d, load_sem.at[i]) for i, (s, d) in enumerate(
        ((vw_hbm, vw), (ow_hbm, ow), (o_hbm, o_ref), (m_hbm, m_ref), (x_hbm, x_ref), (v_hbm, v_ref),
         (vm_hbm, vm), (vs_hbm, vs), (om_hbm, om), (os_hbm, os)))]
    for c_ in own + loads:
        c_.start()
    barrier = pltpu.get_barrier_semaphore()
    near = [p.at(dz, 0, 0) for dz in range(1, a)] + [p.on(p.z, 1, 0), p.on(p.z, 0, 1)]
    for to in near:
        pl.semaphore_signal(barrier, inc=1, device_id={"fs": to}, device_id_type=MESH)
    cores = lax.axis_size("tp")
    siblings = [lax.rem(p.core + d, cores) for d in range(1, cores)]
    for to in siblings:
        pl.semaphore_signal(barrier, inc=1, device_id={"tp": to}, device_id_type=MESH)
    pl.semaphore_wait(barrier, len(near) + len(siblings))
    for c_ in own:
        c_.wait()

    bv, bo = (Bases(p, bases.at[j], b_send.at[j], b_recv.at[j], c_send.at[j], c_recv.at[j]) for j in range(2))
    w0, w1 = (Gather(p, lambda i, ref=ref: ref.at[i], w_send.at[j], w_recv.at[j], line=True, plane_first=first)
              for j, (ref, first) in enumerate(((wv, False), (wo, True))))
    rv, ro = (Scatter(p, part.at[j], code.at[j], got.at[j], r_send.at[j], r_recv.at[j]) for j in range(2))
    lv, lo = (Gather(p, lambda i, j=j: low.at[j, i], l_send.at[j], l_recv.at[j]) for j in range(2))

    depth, rank = bases.shape[2], bases.shape[3]
    high, width = part.shape[2], part.shape[3]
    tokens = x_ref.shape[0]
    tile = math.gcd(tokens, TOKEN_TILE)
    steps = tokens // tile
    far = range(3, a)

    def product(j, start, stop):
        wide, thin = ((x_ref, v_ref), (o_ref, m_ref))[j]

        @pl.loop(start, stop)
        def _(step):
            rows = pl.ds(pl.multiple_of(step * tile, tile), tile)
            thick = jnp.dot(wide[rows, :], bases[j].reshape(n * depth, rank), preferred_element_type=jnp.float32)
            both = jnp.concatenate(halves(thick), axis=0)
            cot = jnp.concatenate([thin[rows, :]] * 2, axis=0)
            part[j] += lax.dot_general(both, cot, FIRST, preferred_element_type=jnp.float32).reshape(n, high, width)

    def pack(j):
        value = part[j, me] * scaling
        low[j, me] = encode(value, (bound(value),) + halves(one(jnp.sum, value * value)), low.shape[2])

    def unpack(j):
        total = jnp.zeros((1, 128), jnp.float32)
        for i in range(n):
            block = low[j, i]
            small[j, i * high:(i + 1) * high] = decode(block, high)[0]
            tail = block[high:].astype(jnp.float32)
            total += tail[1:2, :128] + tail[2:3, :128]
        return total

    def share(total):
        sums[p.core] = jnp.broadcast_to(total, sums.shape[1:])
        out = []
        for d, to in enumerate(siblings):
            out.append(pltpu.make_async_remote_copy(
                src_ref=sums.at[p.core], dst_ref=sums.at[p.core], send_sem=q_send.at[d], recv_sem=q_recv.at[d],
                device_id={"tp": to}, device_id_type=MESH))
            out[-1].start()
        return out

    def shared():
        for d in range(cores - 1):
            ref = sums.at[lax.rem(p.core - d - 1 + cores, cores)]
            pltpu.make_async_remote_copy(
                src_ref=ref, dst_ref=ref, send_sem=q_send.at[d], recv_sem=q_recv.at[d],
                device_id={"tp": p.partner}, device_id_type=MESH).wait_recv()

    def update():
        total = sums[0, :1, :1]
        for i in range(1, cores):
            total += sums[i, :1, :1]
        clip = 1.0 / jnp.sqrt(1.0 + total / entries)
        for scaled, mean, square, mean_next, square_next, norms, at in (
            (clip * small[0], vm, vs, vm_next, vs_next, norms_v, lambda k: (slice(k * rank, (k + 1) * rank), slice(None))),
            (clip * small[1].T, om, os, om_next, os_next, norms_o, lambda k: (slice(None), slice(k * rank, (k + 1) * rank))),
        ):
            mean_new = 0.8 * mean[...] + 0.2 * scaled
            square_new = 0.9 * square[...] + 0.1 * scaled * scaled
            mean_next[...] = mean_new
            square_next[...] = square_new
            for k, part_ in enumerate(halves(mean_new / jnp.sqrt(square_new + 0.1))):
                norms[at(k)] = part_

    def value_steps(basis):
        return jnp.dot(twice(basis), norms_v[...], preferred_element_type=jnp.float32)

    def output_steps(basis):
        return lax.dot_general(norms_o[...], twice(basis), LAST, preferred_element_type=jnp.float32)

    def own_steps():
        v_step[...] = value_steps(bases[0, me])
        v_next[...] = vw[...] - 0.02 * v_step[...]
        o_step[...] = output_steps(bases[1, me])
        o_next[...] = ow[...] - 0.02 * o_step[...]

    def copies(k):
        if k >= a:
            return
        plane = b * c
        count = math.gcd(plane, max(1, BLOCK_LANES // depth))
        span = count * depth

        @pl.loop(0, plane // count)
        def _(i):
            shard = p.planes[k] * plane + i * count
            shards = pl.ds(shard, count)
            to = pl.ds(pl.multiple_of(shard * depth, span), span)
            old = jnp.log2(wv[shards].astype(jnp.float32)).reshape(span, width) * (1.0 / VALUE_RATE)
            v_copy[to, :] = (old - 0.02 * value_steps(bases[0, shards].reshape(span, rank))).astype(v_copy.dtype)
            old = jnp.concatenate([wo[shard + q].astype(jnp.float32) for q in range(count)], axis=1)
            old = jnp.log2(old) * (1.0 / OUTPUT_RATE)
            o_copy[:, to] = (old - 0.02 * output_steps(bases[1, shards].reshape(span, rank))).astype(o_copy.dtype)

    bo.begin_z()
    bo.begin_st()
    bv.begin_z()
    bv.begin_st()
    part[...] = jnp.zeros_like(part)
    for c_ in loads[:2]:
        c_.wait()
    wv[me] = jnp.exp2(VALUE_RATE * vw[...]).astype(wv.dtype)
    wo[me] = jnp.exp2(OUTPUT_RATE * ow[...]).astype(wo.dtype)
    bo.z(1)
    bo.z(2)
    for k in far:
        bo.z(k)
    bo.s(0)
    bo.s(1)
    bo.s(2)
    for k in far:
        bo.s(k)
    bv.z(1)
    bv.z(2)
    for k in far:
        bv.z(k)
    bv.s(0)
    bv.s(1)
    bv.s(2)
    for k in far:
        bv.s(k)
    w0.begin_z()
    w0.begin_st()
    w1.begin_z()
    w1.begin_st()
    bo.last()
    bo.whole()
    for c_ in loads[2:4]:
        c_.wait()
    product(1, 0, steps // 2)
    product(1, steps // 2, steps)
    ro.give_t()
    bv.last()
    bv.whole()
    for c_ in loads[4:6]:
        c_.wait()
    product(0, 0, steps // 2)
    ro.turn_s(0)
    ro.turn_s(1)
    ro.turn_s(2)
    for k in far:
        ro.turn_s(k)
    product(0, steps // 2, steps)
    rv.give_t()
    w0.z(1)
    w0.z(2)
    for k in far:
        w0.z(k)
    w1.near_s()
    w1.z(1)
    w1.z(2)
    ro.turn_z(0)
    ro.turn_z(1)
    ro.turn_z(2)
    for k in far:
        ro.turn_z(k)
    rv.turn_s(0)
    rv.turn_s(1)
    rv.turn_s(2)
    for k in far:
        rv.turn_s(k)
    ro.end()
    pack(1)
    lo.begin_z()
    lo.begin_st()
    rv.turn_z(0)
    rv.turn_z(1)
    rv.turn_z(2)
    for k in far:
        rv.turn_z(k)
    lo.z(1)
    lo.z(2)
    for k in far:
        lo.z(k)
    rv.end()
    pack(0)
    lv.begin_z()
    lv.begin_st()
    w0.s(0)
    w0.s(1)
    w0.s(2)
    for k in far:
        w0.s(k)
    for k in far:
        w1.z(k)
    w1.z(1, 1)
    w1.z(2, 1)
    for k in far:
        w1.z(k, 1)
    lo.s(0)
    lo.s(1)
    lo.s(2)
    for k in far:
        lo.s(k)
    lv.z(1)
    lv.z(2)
    for k in far:
        lv.z(k)
    lo.last()
    total = unpack(1)
    lv.s(0)
    lv.s(1)
    lv.s(2)
    for k in far:
        lv.s(k)
    lv.last()
    total_v = unpack(0)
    sent = share(total + total_v)
    shared()
    for c_ in loads[6:]:
        c_.wait()
    update()
    own_steps()
    w0.t(0)
    w1.t(0)
    copies(0)
    w0.t(1)
    w1.t(1)
    copies(1)
    w0.t(2)
    w1.t(2)
    copies(2)
    for k in far:
        w0.t(k)
    for k in far:
        w1.t(k)
    for k in far:
        copies(k)
    for done in sent:
        done.wait_send()
    for g in (bo, bv, w0, w1, ro, rv, lo, lv):
        g.finish()


def place_out(*refs):
    count = (len(refs) - 1) // 2
    moves = [pltpu.make_async_copy(refs[i], refs[count + i], refs[-1].at[i]) for i in range(count)]
    for move in moves:
        move.start()
    for move in moves:
        move.wait()


def on_device(
    block_input,
    value_cotangent,
    mixed_output,
    output_cotangent,
    value_weight,
    output_weight,
    value_basis,
    output_basis,
    value_mean,
    value_square,
    output_mean,
    output_square,
):
    n, cores = lax.axis_size("fs"), lax.axis_size("tp")
    depth, rank = value_basis.shape
    tokens, width = value_cotangent.shape
    wide = block_input.shape[1]
    a = split_fs(n)[0]
    scaling = 1.0 / math.sqrt(tokens * n)
    entries = 2.0 * rank * width * cores
    f32, b16 = jnp.float32, jnp.bfloat16
    high = rank // n
    rows = (high + 18) // 16 * 16
    hbm = pl.BlockSpec(memory_space=pltpu.HBM)
    vmem = pl.BlockSpec(memory_space=pltpu.VMEM)
    dma = pltpu.SemaphoreType.DMA
    v_row, v_all, v_small = ((depth, width), f32), ((n * depth, width), b16), ((rank, width), f32)
    o_row, o_all, o_small = ((width, depth), f32), ((width, n * depth), b16), ((width, rank), f32)
    outs = (v_row, v_all, v_row, v_small, v_small, o_row, o_all, o_row, o_small, o_small)
    ready = pl.pallas_call(
        functools.partial(exchange, n, scaling, entries),
        out_shape=[pltpu.VMEM(*out) for out in outs],
        in_specs=[hbm] * 12,
        out_specs=[vmem] * len(outs),
        scratch_shapes=[
            pltpu.VMEM((2, n, depth, rank), b16), pltpu.VMEM((n, depth, width), b16), pltpu.VMEM((n, width, depth), b16),
            pltpu.VMEM((2, n, rows, width), b16), pltpu.VMEM((cores, 8, 128), f32),
            pltpu.VMEM((depth, width), f32), pltpu.VMEM((width, depth), f32),
            pltpu.VMEM((tokens, wide), b16), pltpu.VMEM((tokens, width), b16),
            pltpu.VMEM((tokens, width), b16), pltpu.VMEM((tokens, wide), b16),
            pltpu.VMEM((rank, width), f32), pltpu.VMEM((rank, width), f32),
            pltpu.VMEM((width, rank), f32), pltpu.VMEM((width, rank), f32),
            pltpu.VMEM((2, n, high, width), f32), pltpu.VMEM((2, n, rows, width), b16), pltpu.VMEM((2, 4 * a, rows, width), b16),
            pltpu.VMEM((2, rank, width), f32), pltpu.VMEM((2 * rank, width), b16), pltpu.VMEM((width, 2 * rank), b16),
            dma((10,)), dma((2,)),
            dma((2, 4, 2 * a)), dma((2, 4 * a)), dma((2, 4 * a)), dma((2, 4 * a)),
            dma((2, 4, 2 * a)), dma((2, 4 * a)), dma((2, 4, 2 * a)), dma((2, 4 * a)),
            dma((2, 4 * a)), dma((2, 4 * a)), dma((cores,)), dma((cores,)),
        ],
        compiler_params=pltpu.CompilerParams(
            collective_id=0, has_side_effects=True, vmem_limit_bytes=50 * 1024 * 1024),
    )(block_input, value_cotangent, mixed_output, output_cotangent, value_basis, output_basis, value_weight, output_weight,
      value_mean, value_square, output_mean, output_square)
    return tuple(pl.pallas_call(
        place_out,
        out_shape=[jax.ShapeDtypeStruct(*out) for out in outs],
        in_specs=[vmem] * len(outs),
        out_specs=[hbm] * len(outs),
        scratch_shapes=[dma((len(outs),))],
        compiler_params=pltpu.CompilerParams(vmem_limit_bytes=8 * 1024 * 1024),
    )(*ready))


def solution(mesh):
    placed = (
        P("fs", None),
        P("fs", "tp"),
        P("fs", "tp"),
        P("fs", None),
        P("fs", "tp"),
        P("tp", "fs"),
        P("fs", None),
        P("fs", None),
        P(None, "tp"),
        P(None, "tp"),
        P("tp", None),
        P("tp", None),
    )
    return jax.shard_map(
        on_device,
        mesh=mesh,
        in_specs=placed,
        out_specs=(
            P("fs", "tp"),
            P(None, "tp"),
            P("fs", "tp"),
            P(None, "tp"),
            P(None, "tp"),
            P("tp", "fs"),
            P("tp", None),
            P("tp", "fs"),
            P("tp", None),
            P("tp", None),
        ),
        check_vma=False,
    )
```

time: 113 us -> 104 us (0.920)
  the two profiles are of different devices: /device:TPU:9 before, /device:TPU:0 now
where the time goes in v1:
time: 104 us; the launch traced here: 103 us
  Pallas kernels  102 us (98%)
    pallas_call x1, Pallas kernels, on_device(): pl.pallas_call(functools.partial(exchange, n, scaling, entries), out_shap...  99.1 us
    pallas_call x1, Pallas kernels, on_device(): pl.pallas_call(place_out, out_shape=[jax.ShapeDtypeStruct(*out) for out i...  3.38 us

profile of v1, /device:TPU:0, one launch (start us, length us, event | category | flops | bytes accessed | tf_op | source)
XLA Modules:
  0.0 103.2 jit_solution(13517360266555940662)
XLA Ops:
  0.6 99.1 %shard_map.195 = (f32[128,512]{1,0:T(8,128)S(1)}, bf16[2048,512]{1,0:T(8,128)(2,1)S(1)}, f32[128,512]{1,0:T(8,128)S(1)}, f32[384,512]{1,0:T(8,128)S(1)}, f32[384...) custom-call(bf16[1024,2048]{1,0:T(8,128)(2,1)} %x_hbm.1, ...), custom_call_target="tpu_custom_call" | custom-call | tf_op jit(solution)/shard_map/pallas_call | solution.py:590
  99.8 3.4 %shard_map.196 = (f32[128,512]{1,0:T(8,128)}, bf16[2048,512]{1,0:T(8,128)(2,1)}, f32[128,512]{1,0:T(8,128)}, f32[384,512]{1,0:T(8,128)}, f32[384,512]{1,0:T(8,12...) custom-call(f32[128,512]{1,0:T(8,128)S(1)} %get-tuple-element.20.ref, ...), custom_call_target="tpu_custom_call" | custom-call | tf_op jit(solution)/shard_map/pallas_call | solution.py:614

commit v2 on v1

--- a/solution.py
+++ b/solution.py
@@ -12,8 +12,9 @@
 VALUE_RATE = 125.0 / 0.125
 OUTPUT_RATE = 125.0 / 0.1875
 LOW_RATE = 124.0
-BLOCK_LANES = 256
-TOKEN_TILE = 256
+BLOCK_LANES = 512
+LANES = 128
+TOKEN_TILE = 512
 FIRST = (((0,), (0,)), ((), ()))
 LAST = (((1,), (1,)), ((), ()))
 
@@ -158,10 +159,10 @@
 
 
 class Bases(Gather):
-    def __init__(self, place, ref, send, recv, c_send, c_recv):
+    def __init__(self, place, ref, send, recv, c_send, c_recv, plane_first):
         half = ref.shape[1] // 2
         rows = [pl.ds(pl.multiple_of(side * half, half), half) for side in (place.par, 1 - place.par)]
-        super().__init__(place, lambda i: ref.at[i, rows[0]], send, recv, line=False, seen=self.cross)
+        super().__init__(place, lambda i: ref.at[i, rows[0]], send, recv, line=True, plane_first=plane_first, seen=self.cross)
         self.other = lambda i: ref.at[i, rows[1]]
         self.c_send, self.c_recv = c_send, c_recv
         self.crossed = []
@@ -203,16 +204,21 @@
 
 
 def encode(values, entries, rows):
-    row = lax.broadcasted_iota(jnp.int32, (rows - values.shape[0], values.shape[1]), 0)
+    high, width = values.shape
+    pieces = [jnp.exp2((LOW_RATE / entries[0]) * values[:, at:at + LANES]) for at in range(0, width, LANES)]
+    row = lax.broadcasted_iota(jnp.int32, (rows - high * len(pieces), LANES), 0)
     extra = jnp.zeros(row.shape, jnp.float32)
     for k, entry in enumerate(entries):
         extra = jnp.where(row == k, entry.astype(jnp.float32), extra)
-    return jnp.concatenate([jnp.exp2((LOW_RATE / entries[0]) * values), extra], axis=0).astype(jnp.bfloat16)
-
-
-def decode(code, high):
-    top = code[high:high + 1].astype(jnp.float32)
-    return top * (1.0 / LOW_RATE) * jnp.log2(code[:high].astype(jnp.float32)), top
+    return jnp.concatenate(pieces + [extra], axis=0).astype(jnp.bfloat16)
+
+
+def decode(code, high, width):
+    code = code.astype(jnp.float32)
+    end = high * (width // LANES)
+    rate = code[end:end + 1] * (1.0 / LOW_RATE)
+    pieces = [rate * jnp.log2(code[at:at + high]) for at in range(0, end, high)]
+    return jnp.concatenate(pieces, axis=1), code[end:]
 
 
 class Scatter:
@@ -236,16 +242,16 @@
 
     def take(self, block, slot):
         self.copy(block, self.p.me, slot).wait_recv()
-        value, top = decode(self.got[slot], self.part.shape[1])
+        value, tail = decode(self.got[slot], *self.part.shape[1:])
         self.part[block] += value
-        return top.astype(jnp.bfloat16).astype(jnp.float32)
+        return tail[:1]
 
     def grown(self, top):
         return top.astype(jnp.bfloat16).astype(jnp.float32)
 
     def give_t(self):
         n, high, width = self.part.shape
-        self.top = jnp.broadcast_to(bound(self.part[...].reshape(n * high, width)), (1, width))
+        self.top = jnp.broadcast_to(bound(self.part[...].reshape(n * high, width)), (1, LANES))
         for dz in self.order:
             for ds in (1, 0):
                 self.hand(self.p.at(dz, ds, 1), self.p.on(self.p.z, 0, 1), dz * 2 + ds, self.top)
@@ -281,9 +287,33 @@
     return jnp.concatenate([basis, basis], axis=1)
 
 
+def value_steps(basis, norms):
+    return jnp.dot(twice(basis), norms[...], preferred_element_type=jnp.float32)
+
+
+def output_steps(basis, norms):
+    return lax.dot_general(norms[...], twice(basis), LAST, preferred_element_type=jnp.float32)
+
+
+def copy_plane(place, k, bases, wv, wo, norms_v, norms_o, put_v, put_o):
+    depth, rank, width = bases.shape[2], bases.shape[3], wv.shape[2]
+    plane = place.sizes[1] * place.sizes[2]
+    count = math.gcd(plane, max(1, BLOCK_LANES // depth))
+    span = count * depth
+    for i in range(plane // count):
+        shard = place.planes[k] * plane + i * count
+        shards = pl.ds(shard, count)
+        at = pl.ds(i * span, span)
+        old = jnp.log2(wv[shards].astype(jnp.float32)).reshape(span, width) * (1.0 / VALUE_RATE)
+        put_v(at, (old - 0.02 * value_steps(bases[0, shards].reshape(span, rank), norms_v)).astype(jnp.bfloat16))
+        old = jnp.concatenate([wo[shard + q].astype(jnp.float32) for q in range(count)], axis=1)
+        old = jnp.log2(old) * (1.0 / OUTPUT_RATE)
+        put_o(at, (old - 0.02 * output_steps(bases[1, shards].reshape(span, rank), norms_o)).astype(jnp.bfloat16))
+
+
 def exchange(n, scaling, entries, x_hbm, v_hbm, m_hbm, o_hbm, vb_hbm, ob_hbm, vw_hbm, ow_hbm, vm_hbm, vs_hbm, om_hbm, os_hbm,
-             v_next, v_copy, v_step, vm_next, vs_next, o_next, o_copy, o_step, om_next, os_next,
-             bases, wv, wo, low, sums, vw, ow, x_ref, v_ref, m_ref, o_ref, vm, vs, om, os, part, code, got, small, norms_v, norms_o,
+             v_copy, vm_next, vs_next, o_copy, om_next, os_next, bases, wv, wo, vw, ow, norms_v, norms_o,
+             low, sums, x_ref, v_ref, m_ref, o_ref, vm, vs, om, os, part, code, got, small,
              load_sem, own_sem, b_send, b_recv, c_send, c_recv, w_send, w_recv, l_send, l_recv, r_send, r_recv, q_send, q_recv):
     p = Place(n)
     a, b, c = p.sizes
@@ -297,18 +327,24 @@
     for c_ in own + loads:
         c_.start()
     barrier = pltpu.get_barrier_semaphore()
-    near = [p.at(dz, 0, 0) for dz in range(1, a)] + [p.on(p.z, 1, 0), p.on(p.z, 0, 1)]
-    for to in near:
+    for to, inside in ((p.on(p.z + 1, 0, 0), p.z < a - 1), (p.on(p.z - 1, 0, 0), p.z > 0)):
+        @pl.when(inside)
+        def _():
+            pl.semaphore_signal(barrier, inc=1, device_id={"fs": to}, device_id_type=MESH)
+
+    for to in (p.on(p.z, 1, 0), p.on(p.z, 0, 1)):
         pl.semaphore_signal(barrier, inc=1, device_id={"fs": to}, device_id_type=MESH)
+    ends = jnp.where(p.z > 0, 1, 0) + jnp.where(p.z < a - 1, 1, 0)
     cores = lax.axis_size("tp")
     siblings = [lax.rem(p.core + d, cores) for d in range(1, cores)]
     for to in siblings:
         pl.semaphore_signal(barrier, inc=1, device_id={"tp": to}, device_id_type=MESH)
-    pl.semaphore_wait(barrier, len(near) + len(siblings))
+    pl.semaphore_wait(barrier, 2 + len(siblings) + ends)
     for c_ in own:
         c_.wait()
 
-    bv, bo = (Bases(p, bases.at[j], b_send.at[j], b_recv.at[j], c_send.at[j], c_recv.at[j]) for j in range(2))
+    bv, bo = (Bases(p, bases.at[j], b_send.at[j], b_recv.at[j], c_send.at[j], c_recv.at[j], first)
+              for j, first in enumerate((True, False)))
     w0, w1 = (Gather(p, lambda i, ref=ref: ref.at[i], w_send.at[j], w_recv.at[j], line=True, plane_first=first)
               for j, (ref, first) in enumerate(((wv, False), (wo, True))))
     rv, ro = (Scatter(p, part.at[j], code.at[j], got.at[j], r_send.at[j], r_recv.at[j]) for j in range(2))
@@ -337,12 +373,10 @@
         low[j, me] = encode(value, (bound(value),) + halves(one(jnp.sum, value * value)), low.shape[2])
 
     def unpack(j):
-        total = jnp.zeros((1, 128), jnp.float32)
+        total = jnp.zeros((1, LANES), jnp.float32)
         for i in range(n):
-            block = low[j, i]
-            small[j, i * high:(i + 1) * high] = decode(block, high)[0]
-            tail = block[high:].astype(jnp.float32)
-            total += tail[1:2, :128] + tail[2:3, :128]
+            small[j, i * high:(i + 1) * high], tail = decode(low[j, i], high, width)
+            total += tail[1:2] + tail[2:3]
         return total
 
     def share(total):
@@ -378,183 +412,195 @@
             for k, part_ in enumerate(halves(mean_new / jnp.sqrt(square_new + 0.1))):
                 norms[at(k)] = part_
 
-    def value_steps(basis):
-        return jnp.dot(twice(basis), norms_v[...], preferred_element_type=jnp.float32)
-
-    def output_steps(basis):
-        return lax.dot_general(norms_o[...], twice(basis), LAST, preferred_element_type=jnp.float32)
-
-    def own_steps():
-        v_step[...] = value_steps(bases[0, me])
-        v_next[...] = vw[...] - 0.02 * v_step[...]
-        o_step[...] = output_steps(bases[1, me])
-        o_next[...] = ow[...] - 0.02 * o_step[...]
-
     def copies(k):
-        if k >= a:
-            return
-        plane = b * c
-        count = math.gcd(plane, max(1, BLOCK_LANES // depth))
-        span = count * depth
-
-        @pl.loop(0, plane // count)
-        def _(i):
-            shard = p.planes[k] * plane + i * count
-            shards = pl.ds(shard, count)
-            to = pl.ds(pl.multiple_of(shard * depth, span), span)
-            old = jnp.log2(wv[shards].astype(jnp.float32)).reshape(span, width) * (1.0 / VALUE_RATE)
-            v_copy[to, :] = (old - 0.02 * value_steps(bases[0, shards].reshape(span, rank))).astype(v_copy.dtype)
-            old = jnp.concatenate([wo[shard + q].astype(jnp.float32) for q in range(count)], axis=1)
-            old = jnp.log2(old) * (1.0 / OUTPUT_RATE)
-            o_copy[:, to] = (old - 0.02 * output_steps(bases[1, shards].reshape(span, rank))).astype(o_copy.dtype)
-
+        if k < a:
+            span = b * c * depth
+            to = pl.ds(pl.multiple_of(p.planes[k] * span, span), span)
+
+            def put_v(at, value):
+                v_copy.at[to][at, :] = value
+
+            def put_o(at, value):
+                o_copy.at[:, to][:, at] = value
+
+            copy_plane(p, k, bases, wv, wo, norms_v, norms_o, put_v, put_o)
+
+    bv.begin_st()
+    bo.begin_st()
     bo.begin_z()
-    bo.begin_st()
-    bv.begin_z()
-    bv.begin_st()
     part[...] = jnp.zeros_like(part)
     for c_ in loads[:2]:
         c_.wait()
     wv[me] = jnp.exp2(VALUE_RATE * vw[...]).astype(wv.dtype)
     wo[me] = jnp.exp2(OUTPUT_RATE * ow[...]).astype(wo.dtype)
+    w1.begin_st()
+    bv.begin_z()
+    bv.near_s()
     bo.z(1)
     bo.z(2)
-    for k in far:
-        bo.z(k)
-    bo.s(0)
-    bo.s(1)
-    bo.s(2)
-    for k in far:
-        bo.s(k)
     bv.z(1)
     bv.z(2)
+    bv.z(1, 1)
+    bv.z(2, 1)
+    for k in far:
+        bo.z(k)
     for k in far:
         bv.z(k)
-    bv.s(0)
-    bv.s(1)
-    bv.s(2)
-    for k in far:
-        bv.s(k)
+    for k in far:
+        bv.z(k, 1)
     w0.begin_z()
+    w1.begin_z()
+    bo.s(2)
+    bo.s(0)
+    for k in far:
+        bo.s(k)
+    bo.s(1)
+    w1.near_s()
+    bv.last()
     w0.begin_st()
-    w1.begin_z()
-    w1.begin_st()
+    bv.whole()
+    for c_ in loads[4:6]:
+        c_.wait()
+    product(0, 0, steps // 2)
     bo.last()
+    w0.z(1)
+    product(0, steps // 2, steps)
+    rv.give_t()
+    w1.z(1)
+    w0.z(2)
     bo.whole()
     for c_ in loads[2:4]:
         c_.wait()
     product(1, 0, steps // 2)
+    w1.z(2)
     product(1, steps // 2, steps)
     ro.give_t()
-    bv.last()
-    bv.whole()
-    for c_ in loads[4:6]:
-        c_.wait()
-    product(0, 0, steps // 2)
-    ro.turn_s(0)
-    ro.turn_s(1)
-    ro.turn_s(2)
-    for k in far:
-        ro.turn_s(k)
-    product(0, steps // 2, steps)
-    rv.give_t()
-    w0.z(1)
-    w0.z(2)
-    for k in far:
-        w0.z(k)
-    w1.near_s()
-    w1.z(1)
-    w1.z(2)
-    ro.turn_z(0)
-    ro.turn_z(1)
-    ro.turn_z(2)
-    for k in far:
-        ro.turn_z(k)
     rv.turn_s(0)
     rv.turn_s(1)
     rv.turn_s(2)
     for k in far:
+        w0.z(k)
+    for k in far:
         rv.turn_s(k)
+    rv.turn_z(0)
+    w0.s(0)
+    rv.turn_z(1)
+    w1.z(1, 1)
+    rv.turn_z(2)
+    w1.z(2, 1)
+    w0.s(2)
+    w0.s(1)
+    ro.turn_s(0)
+    ro.turn_s(1)
+    for k in far:
+        w1.z(k)
+    ro.turn_s(2)
+    for k in far:
+        ro.turn_s(k)
+    ro.turn_z(0)
+    for k in far:
+        rv.turn_z(k)
+    ro.turn_z(1)
+    ro.turn_z(2)
+    rv.end()
+    for k in far:
+        w1.z(k, 1)
+    w1.t(2)
+    for k in far:
+        ro.turn_z(k)
+    pack(0)
+    for k in far:
+        w0.s(k)
+    lv.begin_z()
+    lv.begin_st()
     ro.end()
     pack(1)
     lo.begin_z()
+    lv.z(1)
+    w1.t(1)
+    w1.t(0)
+    lv.z(2)
     lo.begin_st()
-    rv.turn_z(0)
-    rv.turn_z(1)
-    rv.turn_z(2)
-    for k in far:
-        rv.turn_z(k)
+    for k in far:
+        lv.z(k)
     lo.z(1)
+    lv.s(0)
     lo.z(2)
     for k in far:
         lo.z(k)
-    rv.end()
-    pack(0)
-    lv.begin_z()
-    lv.begin_st()
-    w0.s(0)
-    w0.s(1)
-    w0.s(2)
-    for k in far:
-        w0.s(k)
-    for k in far:
-        w1.z(k)
-    w1.z(1, 1)
-    w1.z(2, 1)
-    for k in far:
-        w1.z(k, 1)
+    lo.s(1)
+    w0.t(0)
+    lv.s(2)
+    lv.s(1)
+    for k in far:
+        lv.s(k)
     lo.s(0)
-    lo.s(1)
+    for k in far:
+        lo.s(k)
     lo.s(2)
     for k in far:
-        lo.s(k)
-    lv.z(1)
-    lv.z(2)
-    for k in far:
-        lv.z(k)
+        w0.t(k)
+    lv.last()
+    total_v = unpack(0)
     lo.last()
     total = unpack(1)
-    lv.s(0)
-    lv.s(1)
-    lv.s(2)
-    for k in far:
-        lv.s(k)
-    lv.last()
-    total_v = unpack(0)
     sent = share(total + total_v)
+    for k in far:
+        w1.t(k)
+    w0.t(2)
+    w0.t(1)
+    for g in (bo, bv, ro, rv, lo, lv):
+        g.finish()
     shared()
+    for done in sent:
+        done.wait_send()
     for c_ in loads[6:]:
         c_.wait()
     update()
-    own_steps()
-    w0.t(0)
-    w1.t(0)
+    copies(1)
     copies(0)
-    w0.t(1)
-    w1.t(1)
-    copies(1)
-    w0.t(2)
-    w1.t(2)
-    copies(2)
-    for k in far:
-        w0.t(k)
-    for k in far:
-        w1.t(k)
-    for k in far:
-        copies(k)
-    for done in sent:
-        done.wait_send()
-    for g in (bo, bv, w0, w1, ro, rv, lo, lv):
+    for g in (w0, w1):
         g.finish()
 
 
-def place_out(*refs):
-    count = (len(refs) - 1) // 2
-    moves = [pltpu.make_async_copy(refs[i], refs[count + i], refs[-1].at[i]) for i in range(count)]
-    for move in moves:
-        move.start()
-    for move in moves:
-        move.wait()
+def finish(early, n, v_copy, vm_ready, vs_ready, o_copy, om_ready, os_ready, bases, wv, wo, vw, ow, norms_v, norms_o,
+           v_next, v_all, v_step, vm_next, vs_next, o_next, o_all, o_step, om_next, os_next,
+           v_new, v_mine, o_new, o_mine, v_late, o_late, sem):
+    p = Place(n)
+    a, b, c = p.sizes
+    span = b * c * bases.shape[2]
+    moves = []
+
+    def move(src, dst):
+        moves.append(pltpu.make_async_copy(src, dst, sem.at[len(moves)]))
+        moves[-1].start()
+
+    def planes(k, v_src, o_src):
+        to = pl.ds(pl.multiple_of(p.planes[k] * span, span), span)
+        move(v_src(to), v_all.at[to])
+        move(o_src(to), o_all.at[:, to])
+
+    for src, dst in ((vm_ready, vm_next), (vs_ready, vs_next), (om_ready, om_next), (os_ready, os_next)):
+        move(src, dst)
+    for k in range(min(early, a)):
+        planes(k, lambda to: v_copy.at[to], lambda to: o_copy.at[:, to])
+    for k in range(early, a):
+        def put_v(at, value):
+            v_late.at[k - early][at, :] = value
+
+        def put_o(at, value):
+            o_late.at[k - early][:, at] = value
+
+        copy_plane(p, k, bases, wv, wo, norms_v, norms_o, put_v, put_o)
+        planes(k, lambda to: v_late.at[k - early], lambda to: o_late.at[k - early])
+    v_mine[...] = value_steps(bases[0, p.me], norms_v)
+    v_new[...] = vw[...] - 0.02 * v_mine[...]
+    o_mine[...] = output_steps(bases[1, p.me], norms_o)
+    o_new[...] = ow[...] - 0.02 * o_mine[...]
+    for src, dst in ((v_mine, v_step), (v_new, v_next), (o_mine, o_step), (o_new, o_next)):
+        move(src, dst)
+    for done in moves:
+        done.wait()
 
 
 def on_device(
@@ -580,44 +626,49 @@
     entries = 2.0 * rank * width * cores
     f32, b16 = jnp.float32, jnp.bfloat16
     high = rank // n
-    rows = (high + 18) // 16 * 16
+    rows = (high * (width // LANES) + 10) // 8 * 8
     hbm = pl.BlockSpec(memory_space=pltpu.HBM)
     vmem = pl.BlockSpec(memory_space=pltpu.VMEM)
     dma = pltpu.SemaphoreType.DMA
     v_row, v_all, v_small = ((depth, width), f32), ((n * depth, width), b16), ((rank, width), f32)
     o_row, o_all, o_small = ((width, depth), f32), ((width, n * depth), b16), ((width, rank), f32)
     outs = (v_row, v_all, v_row, v_small, v_small, o_row, o_all, o_row, o_small, o_small)
+    early = 2
+    span = n // a * depth
+    late = max(a - early, 1)
+    held = (v_all, v_small, v_small, o_all, o_small, o_small, ((2, n, depth, rank), b16), ((n, depth, width), b16),
+            ((n, width, depth), b16), v_row, o_row, ((2 * rank, width), b16), ((width, 2 * rank), b16))
     ready = pl.pallas_call(
         functools.partial(exchange, n, scaling, entries),
-        out_shape=[pltpu.VMEM(*out) for out in outs],
+        out_shape=[pltpu.VMEM(*out) for out in held],
         in_specs=[hbm] * 12,
-        out_specs=[vmem] * len(outs),
+        out_specs=[vmem] * len(held),
         scratch_shapes=[
-            pltpu.VMEM((2, n, depth, rank), b16), pltpu.VMEM((n, depth, width), b16), pltpu.VMEM((n, width, depth), b16),
-            pltpu.VMEM((2, n, rows, width), b16), pltpu.VMEM((cores, 8, 128), f32),
-            pltpu.VMEM((depth, width), f32), pltpu.VMEM((width, depth), f32),
+            pltpu.VMEM((2, n, rows, LANES), b16), pltpu.VMEM((cores, 8, LANES), f32),
             pltpu.VMEM((tokens, wide), b16), pltpu.VMEM((tokens, width), b16),
             pltpu.VMEM((tokens, width), b16), pltpu.VMEM((tokens, wide), b16),
             pltpu.VMEM((rank, width), f32), pltpu.VMEM((rank, width), f32),
             pltpu.VMEM((width, rank), f32), pltpu.VMEM((width, rank), f32),
-            pltpu.VMEM((2, n, high, width), f32), pltpu.VMEM((2, n, rows, width), b16), pltpu.VMEM((2, 4 * a, rows, width), b16),
-            pltpu.VMEM((2, rank, width), f32), pltpu.VMEM((2 * rank, width), b16), pltpu.VMEM((width, 2 * rank), b16),
+            pltpu.VMEM((2, n, high, width), f32), pltpu.VMEM((2, n, rows, LANES), b16), pltpu.VMEM((2, 4 * a, rows, LANES), b16),
+            pltpu.VMEM((2, rank, width), f32),
             dma((10,)), dma((2,)),
             dma((2, 4, 2 * a)), dma((2, 4 * a)), dma((2, 4 * a)), dma((2, 4 * a)),
             dma((2, 4, 2 * a)), dma((2, 4 * a)), dma((2, 4, 2 * a)), dma((2, 4 * a)),
             dma((2, 4 * a)), dma((2, 4 * a)), dma((cores,)), dma((cores,)),
         ],
         compiler_params=pltpu.CompilerParams(
-            collective_id=0, has_side_effects=True, vmem_limit_bytes=50 * 1024 * 1024),
+            collective_id=0, has_side_effects=True, vmem_limit_bytes=40 * 1024 * 1024),
     )(block_input, value_cotangent, mixed_output, output_cotangent, value_basis, output_basis, value_weight, output_weight,
       value_mean, value_square, output_mean, output_square)
     return tuple(pl.pallas_call(
-        place_out,
+        functools.partial(finish, early, n),
         out_shape=[jax.ShapeDtypeStruct(*out) for out in outs],
-        in_specs=[vmem] * len(outs),
+        in_specs=[vmem] * len(held),
         out_specs=[hbm] * len(outs),
-        scratch_shapes=[dma((len(outs),))],
-        compiler_params=pltpu.CompilerParams(vmem_limit_bytes=8 * 1024 * 1024),
+        scratch_shapes=[
+            pltpu.VMEM(*v_row), pltpu.VMEM(*v_row), pltpu.VMEM(*o_row), pltpu.VMEM(*o_row),
+            pltpu.VMEM((late, span, width), b16), pltpu.VMEM((late, width, span), b16), dma((8 + 2 * a,))],
+        compiler_params=pltpu.CompilerParams(vmem_limit_bytes=16 * 1024 * 1024),
     )(*ready))
 
 

time: 104 us -> 79.6 us (0.77)
  Pallas kernels: 102 us -> 78.8 us
    pallas_call x1, Pallas kernels: 99.1 us -> 75.1 us  [on_device(): pl.pallas_call(functools.partial(exchange, n, scaling, entries), out_shap...]
where the time goes in v2:
time: 79.6 us; the launch traced here: 79.5 us
  Pallas kernels  78.8 us (99%)
    pallas_call x1, Pallas kernels, on_device(): pl.pallas_call(functools.partial(exchange, n, scaling, entries), out_shap...  75.1 us
    pallas_call x1, Pallas kernels, on_device(): pl.pallas_call(functools.partial(finish, early, n), out_shape=[jax.ShapeD...  3.73 us

profile of v2, /device:TPU:0, one launch (start us, length us, event | category | flops | bytes accessed | tf_op | source)
XLA Modules:
  0.0 79.5 jit_solution(4856171697868015900)
XLA Ops:
  0.6 75.1 %shard_map.195 = (bf16[2048,512]{1,0:T(8,128)(2,1)S(1)}, f32[384,512]{1,0:T(8,128)S(1)}, f32[384,512]{1,0:T(8,128)S(1)}, bf16[512,2048]{1,0:T(8,128)(2,1)S(1)}, ...) custom-call(bf16[1024,2048]{1,0:T(8,128)(2,1)} %x_hbm.1, ...), custom_call_target="tpu_custom_call" | custom-call | tf_op jit(solution)/shard_map/pallas_call | solution.py:641
  75.7 3.7 %shard_map.196 = (f32[128,512]{1,0:T(8,128)}, bf16[2048,512]{1,0:T(8,128)(2,1)}, f32[128,512]{1,0:T(8,128)}, f32[384,512]{1,0:T(8,128)}, f32[384,512]{1,0:T(8,12...) custom-call(bf16[2048,512]{1,0:T(8,128)(2,1)S(1)} %get-tuple-element, ...), custom_call_target="tpu_custom_call" | custom-call | tf_op jit(solution)/shard_map/pallas_call | solution.py:663

commit v3 on v2

--- a/solution.py
+++ b/solution.py
@@ -425,130 +425,129 @@
 
             copy_plane(p, k, bases, wv, wo, norms_v, norms_o, put_v, put_o)
 
-    bv.begin_st()
     bo.begin_st()
     bo.begin_z()
+    bv.begin_z()
+    bv.begin_st()
     part[...] = jnp.zeros_like(part)
     for c_ in loads[:2]:
         c_.wait()
     wv[me] = jnp.exp2(VALUE_RATE * vw[...]).astype(wv.dtype)
     wo[me] = jnp.exp2(OUTPUT_RATE * ow[...]).astype(wo.dtype)
+    w1.begin_z()
+    w0.begin_st()
+    bo.z(1)
+    bv.near_s()
+    bv.z(1)
+    bo.z(2)
     w1.begin_st()
-    bv.begin_z()
-    bv.near_s()
-    bo.z(1)
-    bo.z(2)
-    bv.z(1)
+    w0.begin_z()
     bv.z(2)
+    bo.s(0)
+    bv.z(2, 1)
+    bo.s(2)
+    for k in far:
+        bo.z(k)
+    bo.s(1)
     bv.z(1, 1)
-    bv.z(2, 1)
-    for k in far:
-        bo.z(k)
+    for k in far:
+        bo.s(k)
     for k in far:
         bv.z(k)
     for k in far:
         bv.z(k, 1)
-    w0.begin_z()
-    w1.begin_z()
-    bo.s(2)
-    bo.s(0)
-    for k in far:
-        bo.s(k)
-    bo.s(1)
+    w1.z(1)
+    w1.z(2)
     w1.near_s()
-    bv.last()
-    w0.begin_st()
-    bv.whole()
-    for c_ in loads[4:6]:
-        c_.wait()
-    product(0, 0, steps // 2)
     bo.last()
     w0.z(1)
-    product(0, steps // 2, steps)
-    rv.give_t()
-    w1.z(1)
-    w0.z(2)
+    bv.last()
     bo.whole()
     for c_ in loads[2:4]:
         c_.wait()
     product(1, 0, steps // 2)
-    w1.z(2)
     product(1, steps // 2, steps)
+    bv.whole()
+    w0.z(2)
     ro.give_t()
+    for c_ in loads[4:6]:
+        c_.wait()
+    product(0, 0, steps // 2)
+    product(0, steps // 2, steps)
+    rv.give_t()
+    w1.z(2, 1)
+    w1.z(1, 1)
+    w0.s(0)
+    ro.turn_s(0)
+    ro.turn_s(1)
+    ro.turn_s(2)
+    for k in far:
+        w1.z(k)
+    for k in far:
+        ro.turn_s(k)
+    ro.turn_z(0)
     rv.turn_s(0)
     rv.turn_s(1)
+    ro.turn_z(1)
+    ro.turn_z(2)
     rv.turn_s(2)
     for k in far:
         w0.z(k)
     for k in far:
         rv.turn_s(k)
     rv.turn_z(0)
-    w0.s(0)
     rv.turn_z(1)
-    w1.z(1, 1)
     rv.turn_z(2)
-    w1.z(2, 1)
-    w0.s(2)
-    w0.s(1)
-    ro.turn_s(0)
-    ro.turn_s(1)
-    for k in far:
-        w1.z(k)
-    ro.turn_s(2)
-    for k in far:
-        ro.turn_s(k)
-    ro.turn_z(0)
-    for k in far:
-        rv.turn_z(k)
-    ro.turn_z(1)
-    ro.turn_z(2)
-    rv.end()
+    for k in far:
+        ro.turn_z(k)
     for k in far:
         w1.z(k, 1)
-    w1.t(2)
-    for k in far:
-        ro.turn_z(k)
-    pack(0)
-    for k in far:
-        w0.s(k)
-    lv.begin_z()
-    lv.begin_st()
     ro.end()
     pack(1)
     lo.begin_z()
+    for k in far:
+        rv.turn_z(k)
+    for k in far:
+        w0.s(k)
+    rv.end()
+    pack(0)
+    lv.begin_z()
+    lo.begin_st()
+    lv.begin_st()
+    lo.z(1)
     lv.z(1)
-    w1.t(1)
+    for k in far:
+        lo.z(k)
     w1.t(0)
+    lo.z(2)
+    lo.s(0)
     lv.z(2)
-    lo.begin_st()
     for k in far:
         lv.z(k)
-    lo.z(1)
-    lv.s(0)
-    lo.z(2)
-    for k in far:
-        lo.z(k)
     lo.s(1)
-    w0.t(0)
-    lv.s(2)
-    lv.s(1)
-    for k in far:
-        lv.s(k)
-    lo.s(0)
     for k in far:
         lo.s(k)
     lo.s(2)
+    lv.s(1)
+    lv.s(2)
+    lv.s(0)
+    for k in far:
+        lv.s(k)
+    w0.s(2)
+    w0.s(1)
+    w1.t(1)
+    w1.t(2)
+    lo.last()
+    w0.t(0)
+    for k in far:
+        w1.t(k)
+    total = unpack(1)
     for k in far:
         w0.t(k)
     lv.last()
     total_v = unpack(0)
-    lo.last()
-    total = unpack(1)
     sent = share(total + total_v)
-    for k in far:
-        w1.t(k)
     w0.t(2)
-    w0.t(1)
     for g in (bo, bv, ro, rv, lo, lv):
         g.finish()
     shared()
@@ -557,8 +556,7 @@
     for c_ in loads[6:]:
         c_.wait()
     update()
-    copies(1)
-    copies(0)
+    w0.t(1)
     for g in (w0, w1):
         g.finish()
 
@@ -633,7 +631,7 @@
     v_row, v_all, v_small = ((depth, width), f32), ((n * depth, width), b16), ((rank, width), f32)
     o_row, o_all, o_small = ((width, depth), f32), ((width, n * depth), b16), ((width, rank), f32)
     outs = (v_row, v_all, v_row, v_small, v_small, o_row, o_all, o_row, o_small, o_small)
-    early = 2
+    early = 0
     span = n // a * depth
     late = max(a - early, 1)
     held = (v_all, v_small, v_small, o_all, o_small, o_small, ((2, n, depth, rank), b16), ((n, depth, width), b16),

time: 79.6 us -> 78.4 us (0.985)
  Pallas kernels: 78.8 us -> 77.6 us
    pallas_call x1, Pallas kernels: 75.1 us -> 72.4 us  [on_device(): pl.pallas_call(functools.partial(exchange, n, scaling, entries), out_shap...]
    pallas_call x1, Pallas kernels: 3.73 us -> 5.19 us  [on_device(): pl.pallas_call(functools.partial(finish, early, n), out_shape=[jax.ShapeD...]
where the time goes in v3:
time: 78.4 us; the launch traced here: 78.2 us
  Pallas kernels  77.6 us (99%)
    pallas_call x1, Pallas kernels, on_device(): pl.pallas_call(functools.partial(exchange, n, scaling, entries), out_shap...  72.4 us
    pallas_call x1, Pallas kernels, on_device(): pl.pallas_call(functools.partial(finish, early, n), out_shape=[jax.ShapeD...  5.19 us

profile of v3, /device:TPU:0, one launch (start us, length us, event | category | flops | bytes accessed | tf_op | source)
XLA Modules:
  0.0 78.2 jit_solution(10538911924406684072)
XLA Ops:
  0.6 72.4 %shard_map.195 = (bf16[2048,512]{1,0:T(8,128)(2,1)S(1)}, f32[384,512]{1,0:T(8,128)S(1)}, f32[384,512]{1,0:T(8,128)S(1)}, bf16[512,2048]{1,0:T(8,128)(2,1)S(1)}, ...) custom-call(bf16[1024,2048]{1,0:T(8,128)(2,1)} %x_hbm.1, ...), custom_call_target="tpu_custom_call" | custom-call | tf_op jit(solution)/shard_map/pallas_call | solution.py:639
  73.0 5.2 %shard_map.196 = (f32[128,512]{1,0:T(8,128)}, bf16[2048,512]{1,0:T(8,128)(2,1)}, f32[128,512]{1,0:T(8,128)}, f32[384,512]{1,0:T(8,128)}, f32[384,512]{1,0:T(8,12...) custom-call(bf16[2048,512]{1,0:T(8,128)(2,1)S(1)} %get-tuple-element, ...), custom_call_target="tpu_custom_call" | custom-call | tf_op jit(solution)/shard_map/pallas_call | solution.py:661
